TPU v7x, 32 devices: a whole 2x2x4 slice. The times are simulated.
32 devices in a mesh: fs: 8 (over z, y), tp: 4 (over x, core).
Axes of the slice: x: 2, y: 2, z: 4, core: 2. Of those that a mesh axis runs over, the one named last changes fastest.
Arguments:
- cotangent: bfloat16 [5120, 1024], P('fs', 'tp'), may hold values from -6 to 6
- inputs: bfloat16 [5120, 1024], P('fs', 'tp'), may hold values from -6 to 6
- pre_act: bfloat16 [5120, 2112], P('fs'), may hold values from -6 to 6
- w_up: bfloat16 [2112, 1024], P('fs', 'tp'), may hold values from -0.1875 to 0.1875
- w_down: bfloat16 [2112, 1024], P('fs', 'tp'), may hold values from -0.125 to 0.125
Outputs:
- grad_input: bfloat16 [5120, 1024], P('fs', 'tp')
- grad_up: float32 [2112, 1024], P('fs', 'tp')
All inputs are finite; a program needn't handle non-finite values.
Results may differ from a plain program's by a relative error of at most 0.0049.
Values may be sent and summed in bfloat16 or wider, within the bound.
A program may use at most 64 MiB of HBM per device.

v0:
```python
import jax
import jax.numpy as jnp
from jax import lax
from jax.sharding import PartitionSpec as P


def times_rows(left, piece):
    return lax.dot_general(
        left, piece, (((1,), (1,)), ((), ())), preferred_element_type=jnp.float32
    )


def local(cotangent, inputs, pre_act, w_up, w_down):
    row_count = cotangent.shape[0]
    token_total = row_count * lax.axis_size("fs")
    full_cotangent = lax.all_gather(cotangent, "tp", axis=1, tiled=True)
    down_whole = lax.all_gather(w_down, "tp", axis=1, tiled=True)
    grad_hidden = times_rows(full_cotangent, lax.all_gather(down_whole, "fs", axis=0, tiled=True))
    grad_pre = (2.0 * grad_hidden * jnp.maximum(pre_act.astype(jnp.float32), 0.0)).astype(
        jnp.bfloat16
    )
    columns = grad_pre
    grad_input = jnp.dot(
        columns, lax.all_gather(w_up, "fs", axis=0, tiled=True), preferred_element_type=jnp.float32
    )
    columns = grad_pre
    grad_share = lax.psum_scatter(
        lax.dot_general(
            columns, inputs, (((0,), (0,)), ((), ())), preferred_element_type=jnp.float32
        ),
        "fs",
        scatter_dimension=0,
        tiled=True,
    )
    grad_up = grad_share / jnp.sqrt(jnp.float32(token_total))
    return (grad_input.astype(jnp.bfloat16), grad_up)


def solution(mesh):
    return jax.shard_map(
        local,
        mesh=mesh,
        in_specs=(P("fs", "tp"), P("fs", "tp"), P("fs", None), P("fs", "tp"), P("fs", "tp")),
        out_specs=(P("fs", "tp"), P("fs", "tp")),
        check_vma=False,
    )
```

profile of v0, /device:TPU:0, one launch (start us, length us, event | category | flops | bytes accessed | tf_op | source)
XLA Modules:
  0.0 227.8 jit_solution(900045571831877215)
XLA Ops:
  7.2 0.0 copy-start
  7.2 0.0 all-gather.4.cloned.1.call-start
  7.2 0.7 all-gather.4.cloned.1.call-update
  7.9 0.0 all-gather.6.cloned.1.call-start
  8.0 10.3 %all_gather.13 = bf16[264,1024]{1,0:T(8,128)(2,1)} all-gather(bf16[264,256]{1,0:T(8,128)(2,1)} %param.9), channel_id=1, replica_groups=mesh['fs'=8,'tp'=4] {'tp'}, dimensions={1}, use_global_device_ids=true | all-gather | bytes 675840 | tf_op jit(solution)/shard_map/all_gather | solution.py:17
  18.3 0.0 all-gather.6.cloned.1.call-update
  18.3 0.0 all-gather.8.cloned.1.call-start
  18.4 0.7 all-gather.8.cloned.1.call-update
  19.1 0.0 reduce-scatter.2.cloned.1.call-start
  19.1 11.5 %all-gather.4.cloned.1.call-done = bf16[640,1024]{1,0:T(8,128)(2,1)} async-done(((bf16[640,256]{1,0:T(8,128)(2,1)}), bf16[640,1024]{1,0:T(8,128)(2,1)}) %all-gather.4.cloned.1.call-update) | async-done | bytes 1310736 | tf_op jit(solution)/shard_map/all_gather | solution.py:16
  30.6 76.6 %all-gather.6.cloned.1.call-done = bf16[2112,1024]{1,0:T(8,128)(2,1)} async-done(((bf16[264,1024]{1,0:T(8,128)(2,1)}), bf16[2112,1024]{1,0:T(8,128)(2,1)}) %all-gather.6.cloned.1.call-update) | async-done | bytes 4325392 | tf_op jit(solution)/shard_map/all_gather | solution.py:18
  107.2 7.1 %fusion.1 = bf16[640,2112]{0,1:T(8,128)(2,1)S(1)} fusion(bf16[640,2112]{0,1:T(8,128)(2,1)} %param.7, bf16[640,1024]{1,0:T(8,128)(2,1)} %all-gather.4.cloned.1.call-done, bf16[2112,1024]{1,0:T(8,128)(2,1)} %all-gather.6.cloned.1.call-done), kind=kOutput, calls=%fused_computation.2 | convolution fusion | flops 2774999040 | bytes 11042816 | tf_op jit(solution)/shard_map/dot_general | solution.py:8
  114.4 0.0 copy-done
  114.4 2.4 %fusion.2 = f32[2112,256]{1,0:T(8,128)} fusion(bf16[640,2112]{0,1:T(8,128)(2,1)S(1)} %fusion.1, bf16[640,256]{1,0:T(8,128)(2,1)S(1)} %copy-done), kind=kOutput, calls=%fused_computation.5 | convolution fusion | flops 692060160 | bytes 5193728 | tf_op jit(solution)/shard_map/dot_general | solution.py:28
  116.7 0.0 reduce-scatter.2.cloned.1.call-update
  116.8 31.7 %all-gather.8.cloned.1.call-done = bf16[2112,256]{1,0:T(8,128)(2,1)} async-done(((bf16[264,256]{1,0:T(8,128)(2,1)}), bf16[2112,256]{1,0:T(8,128)(2,1)}) %all-gather.8.cloned.1.call-update) | async-done | bytes 1081360 | tf_op jit(solution)/shard_map/all_gather | solution.py:24
  148.5 2.9 %convolution_convert_fusion = bf16[640,256]{1,0:T(8,128)(2,1)} fusion(bf16[640,2112]{0,1:T(8,128)(2,1)S(1)} %fusion.1, bf16[2112,256]{1,0:T(8,128)(2,1)} %all-gather.8.cloned.1.call-done), kind=kOutput, calls=%fused_computation.3 | convolution fusion | flops 692224000 | bytes 4112384 | tf_op jit(solution)/shard_map/dot_general | solution.py:23
  151.4 68.2 %reduce-scatter.2.cloned.1.call-done = f32[264,256]{1,0:T(8,128)} async-done(((f32[2112,256]{1,0:T(8,128)}), f32[264,256]{1,0:T(8,128)}) %reduce-scatter.2.cloned.1.call-update) | async-done | bytes 270352 | tf_op jit(solution)/shard_map/reduce_scatter | solution.py:27
  219.6 1.7 broadcast_multiply_fusion
Async XLA Ops:
  7.2 107.2 %copy-start = (bf16[640,256]{1,0:T(8,128)(2,1)S(1)}, bf16[640,256]{1,0:T(8,128)(2,1)}, u32[]{:S(2)}) copy-start(bf16[640,256]{1,0:T(8,128)(2,1)} %param.6) | copy-start | bytes 983044
  7.2 23.4 %all-gather.4.cloned.1.call-start = ((), (), s32[]{:S(2)}) async-start(), calls=%async_computation.1 | async-start | bytes 1638400 | tf_op jit(solution)/shard_map/all_gather | solution.py:16
  7.9 99.3 %all-gather.6.cloned.1.call-start = ((), (), s32[]{:S(2)}) async-start(), calls=%async_computation.2 | async-start | bytes 4866048 | tf_op jit(solution)/shard_map/all_gather | solution.py:18
  18.3 130.1 %all-gather.8.cloned.1.call-start = ((), (), s32[]{:S(2)}) async-start(), calls=%async_computation.3 | async-start | bytes 1216512 | tf_op jit(solution)/shard_map/all_gather | solution.py:24
  19.1 200.5 %reduce-scatter.2.cloned.1.call-start = ((), (), s32[]{:S(2)}) async-start(), calls=%async_computation.4 | async-start | bytes 2433024 | tf_op jit(solution)/shard_map/reduce_scatter | solution.py:27
Sparse Core Ops, SparseCore 0:
  9.5 21.0 all-gather.3
  32.8 74.3 all-gather.5
  109.4 39.0 all-gather.7
  151.8 67.7 reduce-scatter.1
where the time goes:
time: 228 us
  waiting for transfers between devices  189 us (83%)
  between operations  13.8 us (6%)
  matrix products  12.4 us (5%)
  blocking collectives  10.3 us (5%)
    all_gather x1, waiting for transfers between devices, local(): lax.all_gather(down_whole, 'fs', axis=0, tiled=True)  76.6 us
    reduce_scatter x1, waiting for transfers between devices, local(): lax.psum_scatter(lax.dot_general(columns, inputs, (((0,), (0,)), ((), ())...  68.2 us
    all_gather x1, waiting for transfers between devices, local(): lax.all_gather(w_up, 'fs', axis=0, tiled=True)  31.7 us
    all_gather x1, waiting for transfers between devices, local(): full_cotangent = lax.all_gather(cotangent, 'tp', axis=1, tiled=True)  11.5 us
    all_gather x1, blocking collectives, local(): down_whole = lax.all_gather(w_down, 'tp', axis=1, tiled=True)  10.3 us
    dot_general x1, matrix products, times_rows(): lax.dot_general(left, piece, (((1,), (1,)), ((), ())), preferred_element_...  7.12 us
  transfers between devices with their start and end apart: 4, of which 4 were waited for; matrix products, arithmetic and copies ran while one was open for 5% of the time, Pallas kernels for 0%

commit v1 on v0

--- a/solution.py
+++ b/solution.py
@@ -15,7 +15,18 @@
     token_total = row_count * lax.axis_size("fs")
     full_cotangent = lax.all_gather(cotangent, "tp", axis=1, tiled=True)
     down_whole = lax.all_gather(w_down, "tp", axis=1, tiled=True)
-    grad_hidden = times_rows(full_cotangent, lax.all_gather(down_whole, "fs", axis=0, tiled=True))
+    grad_hidden = times_rows(
+        full_cotangent,
+        jnp.concatenate(
+            lax.all_to_all(
+                jnp.stack([down_whole for _ in range(lax.axis_size("fs"))], axis=0),
+                axis_name="fs",
+                split_axis=0,
+                concat_axis=0,
+            ),
+            axis=0,
+        ),
+    )
     grad_pre = (2.0 * grad_hidden * jnp.maximum(pre_act.astype(jnp.float32), 0.0)).astype(
         jnp.bfloat16
     )

time: 228 us -> 220 us (0.965)
  waiting for transfers between devices: 189 us -> 175 us
  starting transfers between devices: 0.16 us -> 5.95 us
  local copies, waits for them, and re-layouts: 0.01 us -> 2.61 us
    all_to_all x0 -> x1, waiting for transfers between devices: none -> 88 us  [local(): lax.all_to_all(jnp.stack([down_whole for _ in range(lax.axis_size('fs'))]...]
    all_gather x1 -> x0, waiting for transfers between devices: 76.6 us -> none  [local(): lax.all_gather(down_whole, 'fs', axis=0, tiled=True)]
    all_gather x1, waiting for transfers between devices: 31.7 us -> 0.02 us  [local(): lax.all_gather(w_up, 'fs', axis=0, tiled=True)]
    all_gather x1, waiting for transfers between devices: 11.5 us -> 20.2 us  [local(): full_cotangent = lax.all_gather(cotangent, 'tp', axis=1, tiled=True)]
    all_to_all x0 -> x1, starting transfers between devices: none -> 5.83 us  [local(): lax.all_to_all(jnp.stack([down_whole for _ in range(lax.axis_size('fs'))]...]
    reduce_scatter x1, waiting for transfers between devices: 68.2 us -> 65 us  [local(): lax.psum_scatter(lax.dot_general(columns, inputs, (((0,), (0,)), ((), ())...]
    another operation x0 -> x1, local copies, waits for them, and re-layouts: none -> 2.6 us  [local(): jnp.stack([down_whole for _ in range(lax.axis_size('fs'))], axis=0)]
  transfers between devices with their start and end apart: 4 -> 4, of which waited for: 4 -> 3; matrix products, arithmetic and copies ran while one was open for 5% -> 6% of each run, Pallas kernels for 0% -> 0%
where the time goes in v1:
time: 220 us
  waiting for transfers between devices  175 us (80%)
  between operations  13.8 us (6%)
  matrix products  12.4 us (6%)
  blocking collectives  9.08 us (4%)
  starting transfers between devices  5.95 us (3%)
  local copies, waits for them, and re-layouts  2.61 us (1%)
    all_to_all x1, waiting for transfers between devices, local(): lax.all_to_all(jnp.stack([down_whole for _ in range(lax.axis_size('fs'))]...  88 us
    reduce_scatter x1, waiting for transfers between devices, local(): lax.psum_scatter(lax.dot_general(columns, inputs, (((0,), (0,)), ((), ())...  65 us
    all_gather x1, waiting for transfers between devices, local(): full_cotangent = lax.all_gather(cotangent, 'tp', axis=1, tiled=True)  20.2 us
    all_gather x1, blocking collectives, local(): down_whole = lax.all_gather(w_down, 'tp', axis=1, tiled=True)  9.08 us
    dot_general x1, matrix products, times_rows(): lax.dot_general(left, piece, (((1,), (1,)), ((), ())), preferred_element_...  7.12 us
    all_to_all x1, starting transfers between devices, local(): lax.all_to_all(jnp.stack([down_whole for _ in range(lax.axis_size('fs'))]...  5.83 us
  transfers between devices with their start and end apart: 4, of which 3 were waited for; matrix products, arithmetic and copies ran while one was open for 6% of the time, Pallas kernels for 0%

profile of v1, /device:TPU:0, one launch (start us, length us, event | category | flops | bytes accessed | tf_op | source)
XLA Modules:
  0.0 220.0 jit_solution(6515564681647642604)
XLA Ops:
  7.2 0.0 copy-start
  7.2 9.1 %all_gather.10 = bf16[264,1024]{1,0:T(8,128)(2,1)S(1)} all-gather(bf16[264,256]{1,0:T(8,128)(2,1)} %param.9), channel_id=1, replica_groups=mesh['fs'=8,'tp'=4] {'tp'}, dimensions={1}, use_global_device_ids=true | all-gather | bytes 675840 | tf_op jit(solution)/shard_map/all_gather | solution.py:17
  16.3 2.6 %stack.2 = bf16[8,264,1024]{2,1,0:T(8,128)(2,1)} broadcast(bf16[264,1024]{1,0:T(8,128)(2,1)S(1)} %all_gather.10), dimensions={1,2} | broadcast | bytes 4866048 | tf_op jit(solution)/shard_map/stack | solution.py:22
  18.9 5.8 %all-to-all-start = ((bf16[8,264,1024]{2,1,0:T(8,128)(2,1)}), bf16[8,264,1024]{2,1,0:T(8,128)(2,1)}, u32[]{:S(2)}, u32[]{:S(2)}) async-start(bf16[8,264,1024]{2,1,0:T(8,128)(2,1)} %stack.2), calls=%async_computation | async-start | bytes 8650752 | tf_op jit(solution)/shard_map/all_to_all | solution.py:21
  24.7 0.0 all-gather.3.cloned.1.call-start
  24.7 0.7 all-gather.3.cloned.1.call-update
  25.4 0.0 all-gather.5.cloned.1.call-start
  25.5 0.7 all-gather.5.cloned.1.call-update
  26.2 0.0 reduce-scatter.2.cloned.1.call-start
  26.2 20.2 %all-gather.3.cloned.1.call-done = bf16[640,1024]{1,0:T(8,128)(2,1)} async-done(((bf16[640,256]{1,0:T(8,128)(2,1)}), bf16[640,1024]{1,0:T(8,128)(2,1)}) %all-gather.3.cloned.1.call-update) | async-done | bytes 1310736 | tf_op jit(solution)/shard_map/all_gather | solution.py:16
  46.4 88.0 %all-to-all-done = bf16[8,264,1024]{2,1,0:T(8,128)(2,1)} async-done(((bf16[8,264,1024]{2,1,0:T(8,128)(2,1)}), bf16[8,264,1024]{2,1,0:T(8,128)(2,1)}, u32[]{:S(2)}, u32[]{:S(2)}) %all-to-all-start) | async-done | bytes 4325408 | tf_op jit(solution)/shard_map/all_to_all | solution.py:21
  134.4 7.1 %fusion.1 = bf16[640,2112]{0,1:T(8,128)(2,1)S(1)} fusion(bf16[640,2112]{0,1:T(8,128)(2,1)} %param.7, bf16[640,1024]{1,0:T(8,128)(2,1)} %all-gather.3.cloned.1.call-done, bf16[2112,1024]{1,0:T(8,128)(2,1)} %bitcast), kind=kOutput, calls=%fused_computation.2 | convolution fusion | flops 2774999040 | bytes 11042816 | tf_op jit(solution)/shard_map/dot_general | solution.py:8
  141.5 0.0 copy-done
  141.5 2.4 %fusion.2 = f32[2112,256]{1,0:T(8,128)} fusion(bf16[640,2112]{0,1:T(8,128)(2,1)S(1)} %fusion.1, bf16[640,256]{1,0:T(8,128)(2,1)S(1)} %copy-done), kind=kOutput, calls=%fused_computation.5 | convolution fusion | flops 692060160 | bytes 5193728 | tf_op jit(solution)/shard_map/dot_general | solution.py:39
  143.9 0.0 reduce-scatter.2.cloned.1.call-update
  143.9 0.0 all-gather.5.cloned.1.call-done
  143.9 2.9 %convolution_convert_fusion = bf16[640,256]{1,0:T(8,128)(2,1)} fusion(bf16[640,2112]{0,1:T(8,128)(2,1)S(1)} %fusion.1, bf16[2112,256]{1,0:T(8,128)(2,1)} %all-gather.5.cloned.1.call-done), kind=kOutput, calls=%fused_computation.3 | convolution fusion | flops 692224000 | bytes 4112384 | tf_op jit(solution)/shard_map/dot_general | solution.py:34
  146.9 65.0 %reduce-scatter.2.cloned.1.call-done = f32[264,256]{1,0:T(8,128)} async-done(((f32[2112,256]{1,0:T(8,128)}), f32[264,256]{1,0:T(8,128)}) %reduce-scatter.2.cloned.1.call-update) | async-done | bytes 270352 | tf_op jit(solution)/shard_map/reduce_scatter | solution.py:38
  211.8 1.7 broadcast_multiply_fusion
Async XLA Ops:
  7.2 134.3 %copy-start = (bf16[640,256]{1,0:T(8,128)(2,1)S(1)}, bf16[640,256]{1,0:T(8,128)(2,1)}, u32[]{:S(2)}) copy-start(bf16[640,256]{1,0:T(8,128)(2,1)} %param.6) | copy-start | bytes 983044
  18.9 115.5 %all-to-all-start = ((bf16[8,264,1024]{2,1,0:T(8,128)(2,1)}), bf16[8,264,1024]{2,1,0:T(8,128)(2,1)}, u32[]{:S(2)}, u32[]{:S(2)}) async-start(bf16[8,264,1024]{2,1,0:T(8,128)(2,1)} %stack.2), calls=%async_computation | async-start | bytes 8650752 | tf_op jit(solution)/shard_map/all_to_all | solution.py:21
  24.7 21.7 %all-gather.3.cloned.1.call-start = ((), (), s32[]{:S(2)}) async-start(), calls=%async_computation.2 | async-start | bytes 1638400 | tf_op jit(solution)/shard_map/all_gather | solution.py:16
  25.4 118.5 %all-gather.5.cloned.1.call-start = ((), (), s32[]{:S(2)}) async-start(), calls=%async_computation.3 | async-start | bytes 1216512 | tf_op jit(solution)/shard_map/all_gather | solution.py:35
  26.2 185.6 %reduce-scatter.2.cloned.1.call-start = ((), (), s32[]{:S(2)}) async-start(), calls=%async_computation.4 | async-start | bytes 2433024 | tf_op jit(solution)/shard_map/reduce_scatter | solution.py:38
Sparse Core Ops, SparseCore 0:
  27.1 19.2 all-gather.2
  48.6 87.0 all-gather.4
  144.0 67.7 reduce-scatter.1
